TPU v7x, 32 devices: a whole 2x2x4 slice. The times are simulated.
32 devices in a mesh: sp: 8 (over z, core), tp: 4 (over y, x).
Axes of the slice: x: 2, y: 2, z: 4, core: 2. Of those that a mesh axis runs over, the one named last changes fastest.
Arguments:
- residual_in: bfloat16 [2048, 2048], P('sp'), may hold values from -6 to 6
- queries: bfloat16 [2048, 2048], P('sp', 'tp'), may hold values from -6 to 4
- keys: bfloat16 [2048, 2048], P('sp', 'tp'), may hold values from -4 to 5.2
- values: bfloat16 [2048, 2048], P('sp', 'tp'), may hold values from -9.5 to 9.5
- out_weight: bfloat16 [2048, 2048], P('tp'), may hold values from -0.125 to 0.125
- norm_gain: float32 [2048], replicated, may hold values from 0.1 to 1.9
- expert_routes: int32 [2048, 2], P('sp'), may hold values from 0 to 7, all different within a row; in each aligned block of 256 rows (0 to 255, 256 to 511, ...) at most 128 rows name the same one
- route_scores: float32 [2048, 2], P('sp'), may hold values from -6 to 6
- gate_weight: bfloat16 [8, 2048, 4096], P('sp', None, 'tp'), may hold values from -0.125 to 0.125
- up_weight: bfloat16 [8, 2048, 4096], P('sp', None, 'tp'), may hold values from -0.125 to 0.125
- down_weight: bfloat16 [8, 4096, 2048], P('sp', 'tp'), may hold values from -0.09375 to 0.09375
Outputs:
- layer_out: bfloat16 [2048, 2048], P('sp', 'tp')
Inputs may be any that keep to these rules, and one draw needn't show every extreme that they name: `expert_routes`: each row names 2 different experts; among the 256 rows of one index of sp no expert is named more than 128 times, and in every draw some such block names some expert exactly 128 times.
All inputs are finite; a program needn't handle non-finite values.
Results may differ from a plain program's by a relative error of at most 0.015.
Values may be sent and summed in bfloat16 or wider, within the bound.
A program may use at most 64 MiB of HBM per device.

v0:
```python
import jax
import jax.numpy as jnp
from jax import lax
from jax.sharding import PartitionSpec as P

HD = 64


epsilon = 1e-06


def attend(queries, query_start, keys_all, values_all):
    row_count = queries.shape[0]
    total_len = keys_all.shape[0]
    head_count = queries.shape[1] // HD
    span = min(512, total_len)
    scale = HD ** (-0.5)
    query_heads = queries.reshape(row_count, head_count, HD)
    query_pos = query_start + lax.iota(jnp.int32, row_count)
    block_count = (query_start + row_count - 1 + span - 1) // span

    def one_block(step_index, state_pair):
        accumulated, kept_log = state_pair
        key_start = (block_count - 1 - step_index) * span
        key_block = lax.dynamic_slice_in_dim(keys_all, key_start, span, 0).reshape(
            span, head_count, HD
        )
        value_block = lax.dynamic_slice_in_dim(values_all, key_start, span, 0).reshape(
            span, head_count, HD
        )
        scores = (
            jnp.einsum("qhc,khc->hqk", query_heads, key_block, preferred_element_type=jnp.float32)
            * scale
        )
        key_pos = key_start + lax.iota(jnp.int32, span)
        causal = key_pos[None, :] < query_pos[:, None]
        log_keep = jnp.where(causal, jax.nn.log_sigmoid(-scores), 0.0)
        between = lax.cumsum(log_keep, axis=2, reverse=True) - log_keep + kept_log[:, :, None]
        weights = jnp.where(causal, jnp.exp(jax.nn.log_sigmoid(scores) + between), 0.0).astype(
            jnp.bfloat16
        )
        accumulated = accumulated + jnp.einsum(
            "hqk,khc->qhc", weights, value_block, preferred_element_type=jnp.float32
        )
        return (accumulated, kept_log + jnp.sum(log_keep, axis=2))

    start_pair = (
        jnp.zeros((row_count, head_count, HD), jnp.float32),
        jnp.zeros((head_count, row_count), jnp.float32),
    )
    accumulated, kept_log = lax.fori_loop(0, block_count, one_block, start_pair)
    return accumulated.reshape(row_count, head_count * HD).astype(jnp.bfloat16)


def route_targets(routes, experts, capacity):
    flat_routes = routes.reshape(-1)
    onehot = (flat_routes[:, None] == lax.iota(jnp.int32, experts)[None, :]).astype(jnp.int32)
    before = jnp.cumsum(onehot, axis=0) - onehot
    return flat_routes * capacity + jnp.sum(before * onehot, axis=1)


def shards(
    residual_in,
    queries,
    keys,
    values,
    out_weight,
    norm_gain,
    expert_routes,
    route_scores,
    gate_weight,
    up_weight,
    down_weight,
):
    row_count = residual_in.shape[0]
    width = residual_in.shape[1]
    row_start = lax.axis_index("sp") * row_count
    keys_all, values_all = (
        lax.all_gather(keys, "sp", axis=0, tiled=True),
        lax.all_gather(values, "sp", axis=0, tiled=True),
    )
    mixed_heads = attend(queries, row_start, keys_all, values_all)
    partial_value = jnp.dot(mixed_heads, out_weight, preferred_element_type=jnp.float32).astype(
        jnp.bfloat16
    )
    attended = lax.psum(partial_value, "tp").astype(jnp.float32).astype(jnp.bfloat16)
    stream = (residual_in.astype(jnp.float32) + attended.astype(jnp.float32)).astype(jnp.bfloat16)
    stream_wide = stream.astype(jnp.float32)
    normed = (
        stream_wide
        * lax.rsqrt(jnp.mean(stream_wide * stream_wide, axis=1, keepdims=True) + epsilon)
        * norm_gain
    ).astype(jnp.bfloat16)
    experts = lax.axis_size("sp")
    capacity = 4 * row_count // experts
    top_count = expert_routes.shape[1]
    targets = route_targets(expert_routes, experts, capacity)
    owners = lax.iota(jnp.int32, row_count * top_count) // top_count
    slot_owner = jnp.full((experts * capacity,), row_count, jnp.int32).at[targets].set(owners)
    padded = jnp.concatenate([normed, jnp.zeros((1, width), jnp.bfloat16)], axis=0)
    outgoing = padded[slot_owner].reshape(experts, capacity, width)
    col_count = width // lax.axis_size("tp")
    column_start = lax.axis_index("tp") * col_count
    own_part = lax.dynamic_slice_in_dim(outgoing, column_start, col_count, 2)
    arrived = lax.all_to_all(own_part, "sp", split_axis=0, concat_axis=0, tiled=True)
    arrived = lax.all_gather(arrived, "tp", axis=2, tiled=True)
    slot_rows = arrived.reshape(-1, width)
    gate_act = jnp.dot(slot_rows, gate_weight[0], preferred_element_type=jnp.float32)
    up_act = jnp.dot(slot_rows, up_weight[0], preferred_element_type=jnp.float32)
    hidden = (jax.nn.silu(gate_act) * up_act).astype(jnp.bfloat16)
    expert_part = (
        jnp.dot(hidden, down_weight[0], preferred_element_type=jnp.float32)
        .astype(jnp.bfloat16)
        .reshape(arrived.shape)
    )
    summed = (
        lax.psum_scatter(expert_part, "tp", scatter_dimension=2, tiled=True)
        .astype(jnp.float32)
        .astype(jnp.bfloat16)
    )
    returned = lax.all_to_all(summed, "sp", split_axis=0, concat_axis=0, tiled=True)
    results = returned.reshape(experts * capacity, col_count)
    picked = results[targets].astype(jnp.float32).reshape(row_count, top_count, col_count)
    shares = jax.nn.sigmoid(route_scores - route_scores[:, ::-1])
    combined = jnp.sum(picked * shares[:, :, None], axis=1)
    own_columns = lax.dynamic_slice_in_dim(stream_wide, column_start, col_count, 1)
    return (own_columns + combined).astype(jnp.bfloat16)


def solution(mesh):
    in_specs = (
        P("sp", None),
        P("sp", "tp"),
        P("sp", "tp"),
        P("sp", "tp"),
        P("tp", None),
        P(),
        P("sp", None),
        P("sp", None),
        P("sp", None, "tp"),
        P("sp", None, "tp"),
        P("sp", "tp", None),
    )
    out_specs = P("sp", "tp")
    return jax.shard_map(shards, mesh=mesh, in_specs=in_specs, out_specs=out_specs, check_vma=False)
```

profile of v0, /device:TPU:0, one launch (start us, length us, event | category | flops | bytes accessed | tf_op | source)
XLA Modules:
  0.0 431.7 jit_solution(17356037483601882176)
XLA Ops:
  6.5 1.9 copy.22
  8.6 1.8 copy.23
  10.4 1.1 copy.24
  11.5 30.8 %all-gather.4.cloned.1.call-done = bf16[2048,512]{0,1:T(8,128)(2,1)} async-done(((bf16[256,512]{0,1:T(8,128)(2,1)}), bf16[2048,512]{0,1:T(8,128)(2,1)}) %all-gather.4.cloned.1.call-update) | async-done | bytes 2097168 | tf_op jit(solution)/shard_map/all_gather | solution.py:80
  42.3 31.2 %all-gather.6.cloned.1.call-done = bf16[2048,512]{0,1:T(8,128)(2,1)} async-done(((bf16[256,512]{0,1:T(8,128)(2,1)}), bf16[2048,512]{0,1:T(8,128)(2,1)}) %all-gather.6.cloned.1.call-update) | async-done | bytes 2097168 | tf_op jit(solution)/shard_map/all_gather | solution.py:79
  73.6 23.8 %while.15 = (s32[]{:T(128)}, f32[256,8,64]{0,2,1:T(8,128)S(1)}, f32[8,256]{1,0:T(8,128)S(1)}, s32[]{:T(128)}, s32[]{:T(128)}, /*index=5*/bf16[2048,512]{0,1:T(8,...) while((s32[]{:T(128)}, f32[256,8,64]{0,2,1:T(8,128)S(1)}, ...), condition=%wide.region_4.5_spmd.clone, body=%wide.region_0.4_spmd.clone.sunk | while | flops 436501248 | bytes 51206344 | solution.py:51
  73.6 1.3 constant_dynamic-slice_fusion.4
  75.1 3.6 fusion.64
  78.7 10.1 %fusion.65 = f32[8,256,4,128]{1,0,3,2:T(8,128)S(1)} fusion(f32[8,256,4,128]{1,3,2,0:T(8,128)S(1)} %bitcast.101), kind=kOutput, calls=%fused_computation.22.clone.1 | output fusion | flops 133169152 | bytes 8388608 | tf_op jit(solution)/shard_map/reduce-window.6
  89.2 1.4 copy.35
  90.6 6.3 %fusion.67 = bf16[8,256,512]{1,2,0:T(8,128)(2,1)S(1)} fusion(f32[8,256,4,128]{1,3,2,0:T(8,128)S(1)} %copy.35, f32[8,512,256]{2,1,0:T(8,128)S(1)} %get-tuple-element.219, f32[8,256]{1,0:T(8,128)S(1)} %get-tuple-element.236, pred[256,512]{0,1:T(8,128)(4,1)S(1)} %broadcast_compare_fusion.2), kind=kLoop, calls=%fused_computation.10.clone.1 | loop fusion | flops 23068672 | bytes 10625024 | tf_op jit(solution)/shard_map/while/body/convert_element_type | solution.py:39
  96.9 0.5 fusion.68
  97.5 1.8 convolution_convert_fusion
  100.1 1.1 reduce-window.24
  101.6 2.6 scatter_custom_fusion
  104.3 117.7 %all-reduce.3.cloned.1.call-done = bf16[256,2048]{1,0:T(8,128)(2,1)} async-done(((bf16[256,2048]{1,0:T(8,128)(2,1)}), bf16[256,2048]{1,0:T(8,128)(2,1)}) %all-reduce.3.cloned.1.call-update) | async-done | bytes 1048592 | tf_op jit(solution)/shard_map/psum | solution.py:86
  222.0 3.0 fusion.30
  225.0 0.5 multiply_convert_fusion.1
  225.6 6.0 %gather_fusion = bf16[1024,2048]{1,0:T(8,128)(2,1)} fusion(bf16[257,2048]{1,0:T(8,128)(2,1)S(1)} %concatenate.3, s32[1024]{0:T(1024)S(1)} %fusion.34), kind=kCustom, calls=%fused_computation | custom fusion | bytes 8392704 | tf_op jit(solution)/shard_map/gather | solution.py:101
  231.6 1.3 constant_dynamic-slice_fusion.2
  233.0 31.1 %all_to_all.10 = bf16[8,128,512]{2,1,0:T(8,128)(2,1)} all-to-all(bf16[8,128,512]{2,1,0:T(8,128)(2,1)S(1)} %constant_dynamic-slice_fusion.2), channel_id=1, replica_groups=mesh['sp'=8,'tp'=4] {'sp'}, dimensions={0} | all-to-all | bytes 2097152 | tf_op jit(solution)/shard_map/all_to_all | solution.py:105
  264.1 50.5 %all-gather.8.cloned.1.call-done = bf16[8,128,2048]{2,1,0:T(8,128)(2,1)} async-done(((bf16[8,128,512]{2,1,0:T(8,128)(2,1)}), bf16[8,128,2048]{2,1,0:T(8,128)(2,1)}) %all-gather.8.cloned.1.call-update) | async-done | bytes 4194320 | tf_op jit(solution)/shard_map/all_gather | solution.py:106
  314.6 7.6 %fusion.21 = f32[1024,1024]{1,0:T(8,128)S(1)} fusion(bf16[1024,2048]{1,0:T(8,128)(2,1)} %bitcast.112, bf16[1,2048,1024]{2,1,0:T(8,128)(2,1)} %param.22), kind=kOutput, calls=%fused_computation.37 | convolution fusion | flops 4294967296 | bytes 12582912 | tf_op jit(solution)/shard_map/dot_general | solution.py:109
  322.3 5.4 %multiply_convert_fusion = bf16[1024,1024]{1,0:T(8,128)(2,1)S(1)} fusion(f32[1024,1024]{1,0:T(8,128)S(1)} %fusion.21, bf16[1024,2048]{1,0:T(8,128)(2,1)S(1)} %bitcast.113, bf16[1,2048,1024]{2,1,0:T(8,128)(2,1)S(1)} %copy-done.6), kind=kOutput, calls=%fused_computation.41 | convolution fusion | flops 4301258752 | bytes 14680064 | tf_op jit(solution)/shard_map/dot_general | solution.py:108
  327.7 6.1 %fusion.25 = bf16[1024,2048]{1,0:T(8,128)(2,1)} fusion(bf16[1024,1024]{1,0:T(8,128)(2,1)S(1)} %multiply_convert_fusion, bf16[1,1024,2048]{2,1,0:T(8,128)(2,1)S(1)} %copy-done.7), kind=kOutput, calls=%fused_computation.42 | convolution fusion | flops 4297064448 | bytes 10485760 | tf_op jit(solution)/shard_map/dot_general | solution.py:112
  333.8 52.7 %reduce-scatter.2.cloned.1.call-done = bf16[8,128,512]{2,1,0:T(8,128)(2,1)} async-done(((bf16[8,128,2048]{2,1,0:T(8,128)(2,1)}), bf16[8,128,512]{2,1,0:T(8,128)(2,1)}) %reduce-scatter.2.cloned.1.call-update) | async-done | bytes 1048592 | tf_op jit(solution)/shard_map/reduce_scatter | solution.py:117
  386.5 4.6 %all-to-all-start.1 = ((bf16[8,128,512]{2,1,0:T(8,128)(2,1)}), bf16[8,128,512]{2,1,0:T(8,128)(2,1)S(1)}, u32[]{:S(2)}, u32[]{:S(2)}) async-start(bf16[8,128,512]{2,1,0:T(8,128)(2,1)} %reduce-scatter.2.cloned.1.call-done), calls=%async_computation.2 | async-start | bytes 2097152 | tf_op jit(solution)/shard_map/all_to_all | solution.py:121
  391.4 26.3 %all-to-all-done.1 = bf16[8,128,512]{2,1,0:T(8,128)(2,1)S(1)} async-done(((bf16[8,128,512]{2,1,0:T(8,128)(2,1)}), bf16[8,128,512]{2,1,0:T(8,128)(2,1)S(1)}, u32[]{:S(2)}, u32[]{:S(2)}) %all-to-all-start.1) | async-done | bytes 1048608 | tf_op jit(solution)/shard_map/all_to_all | solution.py:121
  417.7 2.6 gather_fusion.1
  420.3 1.7 reshape.117
  422.0 1.3 multiply_reduce_fusion.1
  423.3 1.8 add_convert_fusion.1
  (58 shorter events, 2.3 us)
Async XLA Ops:
  6.5 91.0 %copy-start = (bf16[512,2048]{1,0:T(8,128)(2,1)S(1)}, bf16[512,2048]{1,0:T(8,128)(2,1)}, u32[]{:S(2)}) copy-start(bf16[512,2048]{1,0:T(8,128)(2,1)} %param.17) | copy-start | bytes 6291460
  6.5 35.8 %all-gather.4.cloned.1.call-start = ((), (), s32[]{:S(2)}) async-start(), calls=%async_computation.3 | async-start | bytes 2359296 | tf_op jit(solution)/shard_map/all_gather | solution.py:80
  8.5 65.0 %all-gather.6.cloned.1.call-start = ((), (), s32[]{:S(2)}) async-start(), calls=%async_computation.4 | async-start | bytes 2359296 | tf_op jit(solution)/shard_map/all_gather | solution.py:79
  10.4 211.6 %all-reduce.3.cloned.1.call-start = ((), (), s32[]{:S(2)}) async-start(), calls=%async_computation.5 | async-start | bytes 2097152 | tf_op jit(solution)/shard_map/psum | solution.py:86
  97.4 1.9 copy-start.4
  97.5 124.5 %copy-start.1 = (bf16[256,2048]{1,0:T(8,128)(2,1)S(1)}, bf16[256,2048]{1,0:T(8,128)(2,1)}, u32[]{:S(2)}) copy-start(bf16[256,2048]{1,0:T(8,128)(2,1)} %param.13) | copy-start | bytes 3145732
  97.5 127.5 %copy-start.3 = (f32[2048]{0:T(1024)S(1)}, f32[2048]{0:T(1024)}, u32[]{:S(2)}) copy-start(f32[2048]{0:T(1024)} %param.18) | copy-start | bytes 24580
  99.3 215.3 %all-gather.8.cloned.1.call-start = ((), (), s32[]{:S(2)}) async-start(), calls=%async_computation.6 | async-start | bytes 5242880 | tf_op jit(solution)/shard_map/all_gather | solution.py:106
  222.0 3.0 copy-start.2
  264.1 122.4 %reduce-scatter.2.cloned.1.call-start = ((), (), s32[]{:S(2)}) async-start(), calls=%async_computation.7 | async-start | bytes 5242880 | tf_op jit(solution)/shard_map/reduce_scatter | solution.py:117
  314.6 7.7 %copy-start.6 = (bf16[1,2048,1024]{2,1,0:T(8,128)(2,1)S(1)}, bf16[1,2048,1024]{2,1,0:T(8,128)(2,1)}, u32[]{:S(2)}) copy-start(bf16[1,2048,1024]{2,1,0:T(8,128)(2,1)} %param.21) | copy-start | bytes 12582916
  314.6 7.7 %copy-start.8 = (bf16[8,128,2048]{2,1,0:T(8,128)(2,1)S(1)}, bf16[8,128,2048]{2,1,0:T(8,128)(2,1)}, u32[]{:S(2)}) copy-start(bf16[8,128,2048]{2,1,0:T(8,128)(2,1)} %all-gather.8.cloned.1.call-done) | copy-start | bytes 12582916
  322.3 5.4 %copy-start.7 = (bf16[1,1024,2048]{2,1,0:T(8,128)(2,1)S(1)}, bf16[1,1024,2048]{2,1,0:T(8,128)(2,1)}, u32[]{:S(2)}) copy-start(bf16[1,1024,2048]{2,1,0:T(8,128)(2,1)} %param.23) | copy-start | bytes 12582916
  333.7 57.4 %copy-start.5 = (f32[256,2]{0,1:T(2,128)S(1)}, f32[256,2]{0,1:T(2,128)}, u32[]{:S(2)}) copy-start(f32[256,2]{0,1:T(2,128)} %param.20) | copy-start | bytes 6148
  386.5 31.2 %all-to-all-start.1 = ((bf16[8,128,512]{2,1,0:T(8,128)(2,1)}), bf16[8,128,512]{2,1,0:T(8,128)(2,1)S(1)}, u32[]{:S(2)}, u32[]{:S(2)}) async-start(bf16[8,128,512]{2,1,0:T(8,128)(2,1)} %reduce-scatter.2.cloned.1.call-done), calls=%async_computation.2 | async-start | bytes 2097152 | tf_op jit(solution)/shard_map/all_to_all | solution.py:121
Sparse Core Ops, SparseCore 0:
  8.9 33.3 all-gather.3
  43.9 29.6 all-gather.5
  99.4 122.5 all-reduce.2
  264.2 50.3 all-gather.7
  333.9 52.5 reduce-scatter.1
where the time goes:
time: 432 us
  waiting for transfers between devices  309 us (72%)
  blocking collectives  31.1 us (7%)
  matrix products  25 us (6%)
  other arithmetic  24.9 us (6%)
  local copies, waits for them, and re-layouts  23 us (5%)
  between operations  13.4 us (3%)
  starting transfers between devices  4.78 us (1%)
    psum x1, waiting for transfers between devices, shards(): lax.psum(partial_value, 'tp').astype(jnp.float32).astype(jnp.bfloat16)  118 us
    reduce_scatter x1, waiting for transfers between devices, shards(): lax.psum_scatter(expert_part, 'tp', scatter_dimension=2, tiled=True)  52.7 us
    all_gather x1, waiting for transfers between devices, shards(): arrived = lax.all_gather(arrived, 'tp', axis=2, tiled=True)  50.5 us
    all_gather x1, waiting for transfers between devices, shards(): lax.all_gather(keys, 'sp', axis=0, tiled=True)  31.2 us
    all_to_all x1, blocking collectives, shards(): lax.all_to_all(own_part, 'sp', split_axis=0, concat_axis=0, tiled=True)  31.1 us
    all_gather x1, waiting for transfers between devices, shards(): lax.all_gather(values, 'sp', axis=0, tiled=True)  30.8 us
    all_to_all x1, waiting for transfers between devices, shards(): lax.all_to_all(summed, 'sp', split_axis=0, concat_axis=0, tiled=True)  26.3 us
    another operation x4, other arithmetic  11.3 us
  transfers between devices with their start and end apart: 6, of which 6 were waited for; matrix products, arithmetic and copies ran while one was open for 2% of the time, Pallas kernels for 0%

commit v1 on v0

--- a/solution.py
+++ b/solution.py
@@ -1,6 +1,10 @@
+import functools
+
 import jax
 import jax.numpy as jnp
 from jax import lax
+from jax.experimental import pallas as pl
+from jax.experimental.pallas import tpu as pltpu
 from jax.sharding import PartitionSpec as P
 
 HD = 64
@@ -127,6 +131,461 @@
     return (own_columns + combined).astype(jnp.bfloat16)
 
 
+F32 = jnp.float32
+BF16 = jnp.bfloat16
+MESH = pl.DeviceIdType.MESH
+VM = pl.BlockSpec(memory_space=pltpu.VMEM)
+
+
+def dot_f32(left, right, left_dim=1, right_dim=0):
+    return lax.dot_general(
+        left, right, (((left_dim,), (right_dim,)), ((), ())), preferred_element_type=F32
+    )
+
+
+def greet(peers):
+    barrier = pltpu.get_barrier_semaphore()
+    for peer in peers:
+        pl.semaphore_signal(barrier, inc=1, device_id=peer, device_id_type=MESH)
+    pl.semaphore_wait(barrier, len(peers))
+
+
+def attention_kernel(
+    n, q_ref, k_ref, v_ref, out_ref, pack, recv, made, back, send1, recv1, send2, recv2
+):
+    me = lax.axis_index("sp")
+    block = q_ref.shape[0]
+
+    def outward(dst, slot, src):
+        return pltpu.make_async_remote_copy(
+            src_ref=pack.at[dst],
+            dst_ref=recv.at[src],
+            send_sem=send1.at[slot],
+            recv_sem=recv1.at[src],
+            device_id={"sp": dst},
+            device_id_type=MESH,
+        )
+
+    def homeward(dst, src):
+        return pltpu.make_async_remote_copy(
+            src_ref=made.at[dst],
+            dst_ref=back.at[src],
+            send_sem=send2.at[dst],
+            recv_sem=recv2.at[src],
+            device_id={"sp": dst},
+            device_id_type=MESH,
+        )
+
+    scaled = (q_ref[...].astype(F32) * HD ** (-0.5)).astype(BF16)
+    for place, array in enumerate((scaled, k_ref[...], v_ref[...])):
+        turned = array.T
+        for h in range(n):
+            pack[h, place * HD : (place + 1) * HD, :] = turned[h * HD : (h + 1) * HD, :]
+    others = [lax.rem(me + d, n) for d in range(1, n)]
+    greet([{"sp": p} for p in others])
+    for d, dst in enumerate(others):
+        outward(dst, d, me).start()
+    recv[me] = pack[me]
+
+    rows = lax.broadcasted_iota(jnp.int32, (block, block), 0)
+    cols = lax.broadcasted_iota(jnp.int32, (block, block), 1)
+    upper = (cols >= rows).astype(F32).astype(BF16)
+    causal = rows < cols
+
+    def one(i, j, acc, kept, diagonal):
+        q_t = recv[i, 0:HD, :]
+        k_t = recv[j, HD : 2 * HD, :]
+        v_t = recv[j, 2 * HD : 3 * HD, :]
+        z = dot_f32(k_t, q_t, 0, 0)
+        drop = jnp.maximum(z, 0.0) + jnp.log(1.0 + jnp.exp(-jnp.abs(z)))
+        if diagonal:
+            drop = jnp.where(causal, drop, 0.0)
+        high = drop.astype(BF16)
+        low = (drop - high.astype(F32)).astype(BF16)
+        total = dot_f32(upper, high) + dot_f32(upper, low)
+        w = jnp.exp(z - total - kept)
+        if diagonal:
+            w = jnp.where(causal, w, 0.0)
+        acc = acc + dot_f32(v_t, w.astype(BF16))
+        return acc, kept + total[0:1, :]
+
+    for i in range(n):
+
+        @pl.when(me != i)
+        def _():
+            outward(i, 0, i).wait_recv()
+
+        acc = jnp.zeros((HD, block), F32)
+        kept = jnp.zeros((1, block), F32)
+        acc, kept = one(i, i, acc, kept, True)
+        acc, kept = lax.fori_loop(
+            0, i, lambda step, state: one(i, i - 1 - step, state[0], state[1], False), (acc, kept)
+        )
+        made[i] = acc.astype(BF16)
+
+        @pl.when(me != i)
+        def _():
+            homeward(i, me).start()
+
+    back[me] = made[me]
+    for d, dst in enumerate(others):
+        outward(dst, d, me).wait_send()
+        homeward(dst, dst).wait()
+    out_ref[...] = back[...]
+
+
+def attend_by_head(n, queries, keys, values):
+    block = queries.shape[0]
+    return pl.pallas_call(
+        functools.partial(attention_kernel, n),
+        out_shape=jax.ShapeDtypeStruct((n, HD, block), BF16),
+        in_specs=[VM] * 3,
+        out_specs=VM,
+        scratch_shapes=[
+            pltpu.VMEM((n, 3 * HD, block), BF16),
+            pltpu.VMEM((n, 3 * HD, block), BF16),
+            pltpu.VMEM((n, HD, block), BF16),
+            pltpu.VMEM((n, HD, block), BF16),
+            pltpu.SemaphoreType.DMA((n,)),
+            pltpu.SemaphoreType.DMA((n,)),
+            pltpu.SemaphoreType.DMA((n,)),
+            pltpu.SemaphoreType.DMA((n,)),
+        ],
+        compiler_params=pltpu.CompilerParams(collective_id=0, has_side_effects=True),
+    )(queries, keys, values)
+
+
+def expert_kernel(
+    n_sp,
+    n_tp,
+    mixed_ref,
+    ow_ref,
+    res_ref,
+    gain_ref,
+    tgt_rows_ref,
+    tgt_cols_ref,
+    share_ref,
+    gate_hbm,
+    up_hbm,
+    down_hbm,
+    out_ref,
+    gate_w,
+    up_w,
+    down_w,
+    terms,
+    terms_in,
+    sums,
+    sums_in,
+    outgoing,
+    arrived,
+    hidden,
+    parts,
+    parts_in,
+    ret,
+    ret_in,
+    stream_s,
+    w_sem,
+    s_term,
+    r_term,
+    s_sum,
+    r_sum,
+    s_out,
+    r_out,
+    s_ag,
+    r_ag,
+    s_part,
+    r_part,
+    s_ret,
+    r_ret,
+):
+    s, t = lax.axis_index("sp"), lax.axis_index("tp")
+    rows, col = stream_s.shape
+    width = col * n_tp
+    cap = outgoing.shape[0] // n_sp
+    groups = n_sp // 2
+    span = 2 * cap
+    sp_others = [lax.rem(s + d, n_sp) for d in range(1, n_sp)]
+    tp_others = [lax.rem(t + d, n_tp) for d in range(1, n_tp)]
+    loads = [
+        pltpu.make_async_copy(a, b, w_sem.at[i])
+        for i, (a, b) in enumerate(((gate_hbm, gate_w), (up_hbm, up_w), (down_hbm, down_w)))
+    ]
+    for load in loads:
+        load.start()
+
+    def remote(src, dst, send, recv, device):
+        return pltpu.make_async_remote_copy(
+            src_ref=src,
+            dst_ref=dst,
+            send_sem=send,
+            recv_sem=recv,
+            device_id=device,
+            device_id_type=MESH,
+        )
+
+    def term_copy(d):
+        return remote(
+            terms.at[d], terms_in.at[d], s_term.at[d], r_term.at[d], {"tp": tp_others[d]}
+        )
+
+    def sum_copy(d):
+        return remote(sums, sums_in.at[d], s_sum.at[d], r_sum.at[d], {"tp": tp_others[d]})
+
+    def at(start, size):
+        return pl.ds(pl.multiple_of(start, size), size)
+
+    def out_copy(dst, src):
+        return remote(
+            outgoing.at[at(dst * cap, cap)],
+            arrived.at[t, at(src * cap, cap)],
+            s_out.at[dst],
+            r_out.at[src],
+            {"sp": dst},
+        )
+
+    def ag_copy(d, g):
+        piece = arrived.at[t, at(g * span, span)]
+        return remote(piece, piece, s_ag.at[d, g], r_ag.at[d, g], {"tp": tp_others[d]})
+
+    def ag_wait(d, g):
+        piece = arrived.at[lax.rem(t + n_tp - 1 - d, n_tp), at(g * span, span)]
+        remote(piece, piece, s_ag.at[d, g], r_ag.at[d, g], {"tp": tp_others[d]}).wait_recv()
+
+    def part_copy(d, g):
+        return remote(
+            parts.at[d, at(g * span, span)],
+            parts_in.at[d, at(g * span, span)],
+            s_part.at[d, g],
+            r_part.at[d, g],
+            {"tp": tp_others[d]},
+        )
+
+    def ret_copy(dst, src):
+        return remote(
+            ret.at[at(dst * cap, cap)],
+            ret_in.at[at(src * cap, cap)],
+            s_ret.at[dst],
+            r_ret.at[src],
+            {"sp": dst},
+        )
+
+    greet([{"tp": p} for p in tp_others] + [{"sp": p} for p in sp_others])
+    mixed = mixed_ref[...].T
+    for d in range(n_tp - 1):
+        terms[d] = dot_f32(mixed, ow_ref[:, at(tp_others[d] * col, col)]).astype(BF16)
+        term_copy(d).start()
+    attended = dot_f32(mixed, ow_ref[:, at(t * col, col)]).astype(BF16).astype(F32)
+    for d in range(n_tp - 1):
+        term_copy(d).wait_recv()
+        attended = attended + terms_in[d].astype(F32)
+    attended = attended.astype(BF16).astype(F32)
+    stream = (res_ref[:, at(t * col, col)].astype(F32) + attended).astype(BF16).astype(F32)
+    stream_s[...] = stream
+    squares = jnp.sum(stream * stream, axis=1, keepdims=True)
+    sums[...] = jnp.broadcast_to(squares, (rows, 128)).T[0:8, :]
+    for d in range(n_tp - 1):
+        sum_copy(d).start()
+    square_row = sums[0:1, :]
+    for d in range(n_tp - 1):
+        sum_copy(d).wait_recv()
+        square_row = square_row + sums_in[d, 0:1, :]
+    squares = jnp.broadcast_to(square_row, (128, rows)).T[:, 0:1]
+    normed = (
+        stream * lax.rsqrt(squares * (1.0 / width) + epsilon) * gain_ref[0:1, at(t * col, col)]
+    ).astype(BF16)
+    first, second = tgt_rows_ref[0:1, :], tgt_rows_ref[1:2, :]
+    slot_in = lax.broadcasted_iota(jnp.int32, (cap, rows), 0)
+
+    def dispatch(e):
+        slots = slot_in + e * cap
+        pick = ((first == slots) | (second == slots)).astype(F32).astype(BF16)
+        return dot_f32(pick, normed).astype(BF16)
+
+    for dst in sp_others:
+        outgoing[at(dst * cap, cap), :] = dispatch(dst)
+        out_copy(dst, s).start()
+    arrived[t, at(s * cap, cap), :] = dispatch(s)
+    for load in loads:
+        load.wait()
+    chip = s // 2
+
+    def relay(k):
+        g = lax.rem(chip + k, groups)
+        for core in range(2):
+            src = 2 * g + core
+
+            @pl.when(src != s)
+            def _():
+                out_copy(src, src).wait_recv()
+
+        for d in range(n_tp - 1):
+            ag_copy(d, g).start()
+
+    def compute(k):
+        g = lax.rem(chip + k, groups)
+        for d in range(n_tp - 1):
+            ag_wait(d, g)
+        ff = gate_w.shape[1]
+        tile = min(256, ff)
+        here = at(g * span, span)
+
+        def hidden_tile(i, carry):
+            lanes = at(i * tile, tile)
+            gate_act = jnp.zeros((span, tile), F32)
+            up_act = jnp.zeros((span, tile), F32)
+            for c in range(n_tp):
+                x = arrived[c, here, :]
+                gate_act = gate_act + dot_f32(x, gate_w[c * col : (c + 1) * col, lanes])
+                up_act = up_act + dot_f32(x, up_w[c * col : (c + 1) * col, lanes])
+            act = gate_act / (1.0 + jnp.exp(-gate_act)) * up_act
+            hidden[:, lanes] = act.astype(BF16)
+            return carry
+
+        lax.fori_loop(0, ff // tile, hidden_tile, 0)
+        for d in range(n_tp - 1):
+            parts[d, here, :] = dot_f32(
+                hidden[...], down_w[:, at(tp_others[d] * col, col)]
+            ).astype(BF16)
+            part_copy(d, g).start()
+        parts[n_tp - 1, here, :] = dot_f32(hidden[...], down_w[:, at(t * col, col)]).astype(BF16)
+
+    def finish(k):
+        g = lax.rem(chip + k, groups)
+        here = at(g * span, span)
+        total = parts[n_tp - 1, here, :].astype(F32)
+        for d in range(n_tp - 1):
+            part_copy(d, g).wait_recv()
+            total = total + parts_in[d, here, :].astype(F32)
+        ret[here, :] = total.astype(BF16)
+        for core in range(2):
+            src = 2 * g + core
+
+            @pl.when(src != s)
+            def _():
+                ret_copy(src, s).start()
+
+    relay(0)
+
+    def step(k, carry):
+        @pl.when(k + 1 < groups)
+        def _():
+            relay(k + 1)
+
+        compute(k)
+
+        @pl.when(k > 0)
+        def _():
+            finish(k - 1)
+
+        return carry
+
+    lax.fori_loop(0, groups, step, 0)
+    finish(groups - 1)
+    ret_in[at(s * cap, cap), :] = ret[at(s * cap, cap), :]
+    for dst in sp_others:
+        ret_copy(dst, dst).wait_recv()
+    slots = lax.broadcasted_iota(jnp.int32, (rows, n_sp * cap), 1)
+    total = jnp.zeros((rows, col), F32)
+    for k in range(2):
+        pick = (tgt_cols_ref[:, k : k + 1] == slots).astype(F32).astype(BF16)
+        other = share_ref[:, 1 - k : 2 - k]
+        share = 1.0 / (1.0 + jnp.exp(other - share_ref[:, k : k + 1]))
+        total = total + dot_f32(pick, ret_in[...]) * share
+    out_ref[...] = (stream_s[...] + total).astype(BF16)
+    for d in range(n_tp - 1):
+        term_copy(d).wait_send()
+        sum_copy(d).wait_send()
+    for dst in sp_others:
+        out_copy(dst, s).wait_send()
+        ret_copy(dst, s).wait_send()
+
+    def drain(g, carry):
+        for d in range(n_tp - 1):
+            ag_copy(d, g).wait_send()
+            part_copy(d, g).wait_send()
+        return carry
+
+    lax.fori_loop(0, groups, drain, 0)
+
+
+def fused_shards(
+    n_sp,
+    n_tp,
+    residual_in,
+    queries,
+    keys,
+    values,
+    out_weight,
+    norm_gain,
+    expert_routes,
+    route_scores,
+    gate_weight,
+    up_weight,
+    down_weight,
+):
+    rows, width = residual_in.shape
+    col = width // n_tp
+    cap = 4 * rows // n_sp
+    slots = n_sp * cap
+    ff = gate_weight.shape[2]
+    mixed = attend_by_head(n_sp, queries, keys, values).reshape(n_sp * HD, rows)
+    targets = route_targets(expert_routes, n_sp, cap).reshape(rows, 2)
+    anywhere = pl.BlockSpec(memory_space=pl.ANY)
+    dma = pltpu.SemaphoreType.DMA
+    far = n_tp - 1
+    groups = n_sp // 2
+    return pl.pallas_call(
+        functools.partial(expert_kernel, n_sp, n_tp),
+        out_shape=jax.ShapeDtypeStruct((rows, col), BF16),
+        in_specs=[VM] * 7 + [anywhere] * 3,
+        out_specs=VM,
+        scratch_shapes=[
+            pltpu.VMEM((width, ff), BF16),
+            pltpu.VMEM((width, ff), BF16),
+            pltpu.VMEM((ff, width), BF16),
+            pltpu.VMEM((far, rows, col), BF16),
+            pltpu.VMEM((far, rows, col), BF16),
+            pltpu.VMEM((8, rows), F32),
+            pltpu.VMEM((far, 8, rows), F32),
+            pltpu.VMEM((slots, col), BF16),
+            pltpu.VMEM((n_tp, slots, col), BF16),
+            pltpu.VMEM((2 * cap, ff), BF16),
+            pltpu.VMEM((n_tp, slots, col), BF16),
+            pltpu.VMEM((far, slots, col), BF16),
+            pltpu.VMEM((slots, col), BF16),
+            pltpu.VMEM((slots, col), BF16),
+            pltpu.VMEM((rows, col), F32),
+            dma((3,)),
+            dma((far,)),
+            dma((far,)),
+            dma((far,)),
+            dma((far,)),
+            dma((n_sp,)),
+            dma((n_sp,)),
+            dma((far, groups)),
+            dma((far, groups)),
+            dma((far, groups)),
+            dma((far, groups)),
+            dma((n_sp,)),
+            dma((n_sp,)),
+        ],
+        compiler_params=pltpu.CompilerParams(
+            collective_id=1, has_side_effects=True, vmem_limit_bytes=60 * 1024 * 1024
+        ),
+    )(
+        mixed,
+        out_weight,
+        residual_in,
+        norm_gain.reshape(1, width),
+        targets.T,
+        targets,
+        route_scores,
+        gate_weight[0],
+        up_weight[0],
+        down_weight[0],
+    )
+
+
 def solution(mesh):
     in_specs = (
         P("sp", None),
@@ -142,4 +601,12 @@
         P("sp", "tp", None),
     )
     out_specs = P("sp", "tp")
-    return jax.shard_map(shards, mesh=mesh, in_specs=in_specs, out_specs=out_specs, check_vma=False)
+    n_sp, n_tp = mesh.shape["sp"], mesh.shape["tp"]
+
+    def body(*args):
+        heads = args[1].shape[1] // HD
+        if heads == n_sp:
+            return fused_shards(n_sp, n_tp, *args)
+        return shards(*args)
+
+    return jax.shard_map(body, mesh=mesh, in_specs=in_specs, out_specs=out_specs, check_vma=False)

time: 432 us -> 189 us (0.44)
  waiting for transfers between devices: 309 us -> 0 us
  Pallas kernels: 0 us -> 179 us
  blocking collectives: 31.1 us -> 0 us
  matrix products: 25 us -> 0 us
  other arithmetic: 24.9 us -> 1.98 us
  local copies, waits for them, and re-layouts: 23 us -> 5.37 us
  between operations: 13.4 us -> 0.08 us
  starting transfers between devices: 4.78 us -> 0 us
    pallas_call x0 -> x2, Pallas kernels: none -> 179 us  [the longest x1 141 us: fused_shards(): pl.pallas_call(functools.partial(expert_kernel, n_sp, n_tp), out_shape=ja...]
    psum x1 -> x0, waiting for transfers between devices: 118 us -> none  [shards(): lax.psum(partial_value, 'tp').astype(jnp.float32).astype(jnp.bfloat16)]
    all_gather x3 -> x0, waiting for transfers between devices: 113 us -> none  [the longest x1 50.5 us: shards(): arrived = lax.all_gather(arrived, 'tp', axis=2, tiled=True)]
    reduce_scatter x1 -> x0, waiting for transfers between devices: 52.7 us -> none  [shards(): lax.psum_scatter(expert_part, 'tp', scatter_dimension=2, tiled=True)]
    all_to_all x1 -> x0, blocking collectives: 31.1 us -> none  [shards(): lax.all_to_all(own_part, 'sp', split_axis=0, concat_axis=0, tiled=True)]
    all_to_all x1 -> x0, waiting for transfers between devices: 26.3 us -> none  [shards(): lax.all_to_all(summed, 'sp', split_axis=0, concat_axis=0, tiled=True)]
    dot_general x6 -> x0, matrix products: 25 us -> none  [the longest x1 7.64 us: shards(): jnp.dot(slot_rows, up_weight[0], preferred_element_type=jnp.float32)]
    convert_element_type x5 -> x0, other arithmetic: 11.6 us -> none  [the longest x1 6.33 us: one_block(): jnp.where(causal, jnp.exp(jax.nn.log_sigmoid(scores) + between), 0.0)]
  transfers between devices with their start and end apart: 6 -> 0, of which waited for: 6 -> 0; matrix products, arithmetic and copies ran while one was open for 2% -> 0% of each run, Pallas kernels for 0% -> 0%
where the time goes in v1:
time: 189 us; the launch traced here: 187 us
  Pallas kernels  179 us (95%)
  local copies, waits for them, and re-layouts  5.37 us (3%)
  other arithmetic  1.98 us (1%)
    pallas_call x1, Pallas kernels, fused_shards(): pl.pallas_call(functools.partial(expert_kernel, n_sp, n_tp), out_shape=ja...  141 us
    pallas_call x1, Pallas kernels, attend_by_head(): pl.pallas_call(functools.partial(attention_kernel, n), out_shape=jax.Shap...  38.5 us
    unnamed x5, local copies, waits for them, and re-layouts  3.96 us

profile of v1, /device:TPU:0, one launch (start us, length us, event | category | flops | bytes accessed | tf_op | source)
XLA Modules:
  0.0 186.6 jit_solution(9322408630548784668)
XLA Ops:
  0.0 0.7 broadcast_multiply_fusion
  0.7 0.1 copy.24
  0.8 0.8 copy.22
  1.6 0.1 eq.29
  1.8 0.1 eq.25
  2.0 1.1 reduce-window.6
  3.1 0.2 slice_reduce_fusion
  3.4 0.1 fusion.1
  3.4 0.1 reduce_sum.12
  3.6 0.0 copy-start
  3.6 0.6 copy.25.tgt_rows_ref
  4.3 1.5 copy.26.share_ref
  5.7 38.5 %shard_map.109 = bf16[8,64,256]{2,1,0:T(8,128)(2,1)} custom-call(bf16[256,512]{1,0:T(8,128)(2,1)} %q_ref.1, bf16[256,512]{1,0:T(8,128)(2,1)} %k_ref.1, bf16[256,512]{1,0:T(8,128)(2,1)} %v_ref.1), custom_call_target="tpu_custom_call" | custom-call | tf_op jit(solution)/shard_map/pallas_call | solution.py:239
  44.2 0.0 copy-done
  44.2 140.7 %shard_map.110 = bf16[256,512]{1,0:T(8,128)(2,1)} custom-call(bf16[512,256]{1,0:T(8,128)(2,1)} %bitcast.18, bf16[512,2048]{1,0:T(8,128)(2,1)} %ow_ref.1, bf16[256,2048]{1,0:T(8,128)(2,1)} %res_ref.1, f32[1,2048]{1,0:T(1,128)} %bitcast.19, s32[2,256]{1,0:T(2,128)} %copy.25.tgt_rows_ref, s32[256,2]{1,0:T(8,128)} %copy-done, f32[256,2]{1,0:T(8,128)} %copy.26.share_ref, ...), custom_call_target="tpu_custom_call" | custom-call | tf_op jit(solution)/shard_map/pallas_call | solution.py:537
  185.0 1.7 copy.28
  (4 shorter events, 0.1 us)
Async XLA Ops:
  3.6 40.6 %copy-start = (s32[256,2]{1,0:T(8,128)}, s32[256,2]{1,0:T(8,128)S(1)}, u32[]{:S(2)}) copy-start(s32[256,2]{1,0:T(8,128)S(1)} %add.4.tgt_cols_ref) | copy-start | bytes 6148

commit v2 on v1

--- a/solution.py
+++ b/solution.py
@@ -151,7 +151,7 @@
 
 
 def attention_kernel(
-    n, q_ref, k_ref, v_ref, out_ref, pack, recv, made, back, send1, recv1, send2, recv2
+    n, q_ref, k_ref, v_ref, pack, recv, made, back, send1, recv1, send2, recv2
 ):
     me = lax.axis_index("sp")
     block = q_ref.shape[0]
@@ -182,7 +182,6 @@
         for h in range(n):
             pack[h, place * HD : (place + 1) * HD, :] = turned[h * HD : (h + 1) * HD, :]
     others = [lax.rem(me + d, n) for d in range(1, n)]
-    greet([{"sp": p} for p in others])
     for d, dst in enumerate(others):
         outward(dst, d, me).start()
     recv[me] = pack[me]
@@ -215,13 +214,17 @@
         def _():
             outward(i, 0, i).wait_recv()
 
-        acc = jnp.zeros((HD, block), F32)
-        kept = jnp.zeros((1, block), F32)
-        acc, kept = one(i, i, acc, kept, True)
-        acc, kept = lax.fori_loop(
-            0, i, lambda step, state: one(i, i - 1 - step, state[0], state[1], False), (acc, kept)
-        )
-        made[i] = acc.astype(BF16)
+        state = one(i, i, jnp.zeros((HD, block), F32), jnp.zeros((1, block), F32), True)
+        odd = i % 2
+        if odd:
+            state = one(i, i - 1, *state, False)
+
+        def pair(step, state):
+            j = i - 1 - odd - 2 * step
+            return one(i, j - 1, *one(i, j, *state, False), False)
+
+        state = lax.fori_loop(0, i // 2, pair, state)
+        made[i] = state[0].astype(BF16)
 
         @pl.when(me != i)
         def _():
@@ -231,44 +234,33 @@
     for d, dst in enumerate(others):
         outward(dst, d, me).wait_send()
         homeward(dst, dst).wait()
-    out_ref[...] = back[...]
-
-
-def attend_by_head(n, queries, keys, values):
-    block = queries.shape[0]
-    return pl.pallas_call(
-        functools.partial(attention_kernel, n),
-        out_shape=jax.ShapeDtypeStruct((n, HD, block), BF16),
-        in_specs=[VM] * 3,
-        out_specs=VM,
-        scratch_shapes=[
-            pltpu.VMEM((n, 3 * HD, block), BF16),
-            pltpu.VMEM((n, 3 * HD, block), BF16),
-            pltpu.VMEM((n, HD, block), BF16),
-            pltpu.VMEM((n, HD, block), BF16),
-            pltpu.SemaphoreType.DMA((n,)),
-            pltpu.SemaphoreType.DMA((n,)),
-            pltpu.SemaphoreType.DMA((n,)),
-            pltpu.SemaphoreType.DMA((n,)),
-        ],
-        compiler_params=pltpu.CompilerParams(collective_id=0, has_side_effects=True),
-    )(queries, keys, values)
 
 
 def expert_kernel(
     n_sp,
     n_tp,
-    mixed_ref,
-    ow_ref,
-    res_ref,
+    q_ref,
+    k_ref,
+    v_ref,
+    routes_ref,
+    scores_ref,
     gain_ref,
-    tgt_rows_ref,
-    tgt_cols_ref,
-    share_ref,
+    ow_hbm,
+    res_hbm,
     gate_hbm,
     up_hbm,
     down_hbm,
     out_ref,
+    pack,
+    recv,
+    made,
+    back,
+    send1,
+    recv1,
+    send2,
+    recv2,
+    ow_ref,
+    res_ref,
     gate_w,
     up_w,
     down_w,
@@ -280,6 +272,7 @@
     arrived,
     hidden,
     parts,
+    mid,
     parts_in,
     ret,
     ret_in,
@@ -293,6 +286,10 @@
     r_out,
     s_ag,
     r_ag,
+    s_fw,
+    r_fw,
+    s_mid,
+    r_mid,
     s_part,
     r_part,
     s_ret,
@@ -304,12 +301,26 @@
     cap = outgoing.shape[0] // n_sp
     groups = n_sp // 2
     span = 2 * cap
+    chip = s // 2
     sp_others = [lax.rem(s + d, n_sp) for d in range(1, n_sp)]
-    tp_others = [lax.rem(t + d, n_tp) for d in range(1, n_tp)]
-    loads = [
-        pltpu.make_async_copy(a, b, w_sem.at[i])
-        for i, (a, b) in enumerate(((gate_hbm, gate_w), (up_hbm, up_w), (down_hbm, down_w)))
-    ]
+    beside = t + 1 - 2 * lax.rem(t, 2)
+    across = t + 2 - 4 * (t // 2)
+    corner = 3 - t
+    peers = [beside, across, corner]
+    far = len(peers)
+
+    def at(start, size):
+        return pl.ds(pl.multiple_of(start, size), size)
+
+    own = at(t * col, col)
+    pairs = (
+        (ow_hbm, ow_ref),
+        (res_hbm.at[:, own], res_ref),
+        (gate_hbm, gate_w),
+        (up_hbm, up_w),
+        (down_hbm, down_w),
+    )
+    loads = [pltpu.make_async_copy(a, b, w_sem.at[i]) for i, (a, b) in enumerate(pairs)]
     for load in loads:
         load.start()
 
@@ -324,15 +335,10 @@
         )
 
     def term_copy(d):
-        return remote(
-            terms.at[d], terms_in.at[d], s_term.at[d], r_term.at[d], {"tp": tp_others[d]}
-        )
+        return remote(terms.at[d], terms_in.at[d], s_term.at[d], r_term.at[d], {"tp": peers[d]})
 
     def sum_copy(d):
-        return remote(sums, sums_in.at[d], s_sum.at[d], r_sum.at[d], {"tp": tp_others[d]})
-
-    def at(start, size):
-        return pl.ds(pl.multiple_of(start, size), size)
+        return remote(sums, sums_in.at[d], s_sum.at[d], r_sum.at[d], {"tp": peers[d]})
 
     def out_copy(dst, src):
         return remote(
@@ -343,21 +349,31 @@
             {"sp": dst},
         )
 
-    def ag_copy(d, g):
-        piece = arrived.at[t, at(g * span, span)]
-        return remote(piece, piece, s_ag.at[d, g], r_ag.at[d, g], {"tp": tp_others[d]})
-
-    def ag_wait(d, g):
-        piece = arrived.at[lax.rem(t + n_tp - 1 - d, n_tp), at(g * span, span)]
-        remote(piece, piece, s_ag.at[d, g], r_ag.at[d, g], {"tp": tp_others[d]}).wait_recv()
-
-    def part_copy(d, g):
+    def ag_copy(d, g, owner):
+        piece = arrived.at[owner, at(g * span, span)]
+        return remote(piece, piece, s_ag.at[d, g], r_ag.at[d, g], {"tp": peers[d]})
+
+    def fw_copy(d, g, owner):
+        piece = arrived.at[owner, at((2 * g + d) * cap, cap)]
+        return remote(piece, piece, s_fw.at[d, g], r_fw.at[d, g], {"tp": peers[1 - d]})
+
+    def mid_copy(d, g):
         return remote(
-            parts.at[d, at(g * span, span)],
-            parts_in.at[d, at(g * span, span)],
-            s_part.at[d, g],
-            r_part.at[d, g],
-            {"tp": tp_others[d]},
+            parts.at[3, at((2 * g + d) * cap, cap)],
+            mid.at[d, at(g * cap, cap)],
+            s_mid.at[d, g],
+            r_mid.at[d, g],
+            {"tp": peers[d]},
+        )
+
+    def part_copy(d, half, g):
+        here = at((2 * g + half) * cap, cap)
+        return remote(
+            parts.at[1 + d, here],
+            parts_in.at[d, here],
+            s_part.at[d, half, g],
+            r_part.at[d, half, g],
+            {"tp": peers[d]},
         )
 
     def ret_copy(dst, src):
@@ -369,48 +385,73 @@
             {"sp": dst},
         )
 
-    greet([{"tp": p} for p in tp_others] + [{"sp": p} for p in sp_others])
-    mixed = mixed_ref[...].T
-    for d in range(n_tp - 1):
-        terms[d] = dot_f32(mixed, ow_ref[:, at(tp_others[d] * col, col)]).astype(BF16)
+    greet([{"tp": p} for p in peers] + [{"sp": p} for p in sp_others])
+    attention_kernel(
+        n_sp, q_ref, k_ref, v_ref, pack, recv, made, back, send1, recv1, send2, recv2
+    )
+    loads[0].wait()
+    loads[1].wait()
+    mixed = back[...].reshape(n_sp * HD, rows).T
+    for d in (2, 0, 1):
+        terms[d] = dot_f32(mixed, ow_ref[:, at(peers[d] * col, col)]).astype(BF16)
         term_copy(d).start()
-    attended = dot_f32(mixed, ow_ref[:, at(t * col, col)]).astype(BF16).astype(F32)
-    for d in range(n_tp - 1):
+    attended = dot_f32(mixed, ow_ref[:, own]).astype(BF16).astype(F32)
+
+    routes = routes_ref[...].astype(F32)
+    turned = [jnp.broadcast_to(routes[k : k + 1, :], (128, rows)).T for k in range(2)]
+    lane = lax.broadcasted_iota(jnp.int32, (rows, 128), 1).astype(F32)
+    named = [(column == lane).astype(F32) for column in turned]
+    row_of = lax.broadcasted_iota(jnp.int32, (rows, rows), 0)
+    col_of = lax.broadcasted_iota(jnp.int32, (rows, rows), 1)
+    earlier = (col_of < row_of).astype(F32).astype(BF16)
+    before = dot_f32(earlier, (named[0] + named[1]).astype(BF16))
+    tgt_cols, tgt_rows = [], []
+    for k in range(2):
+        slot = jnp.sum(before * named[k], axis=1, keepdims=True)
+        target = turned[k] * float(cap) + slot
+        tgt_cols.append(target[:, 0:1].astype(jnp.int32))
+        tgt_rows.append(target.T[0:1, :].astype(jnp.int32))
+
+    for d in (0, 1, 2):
         term_copy(d).wait_recv()
         attended = attended + terms_in[d].astype(F32)
     attended = attended.astype(BF16).astype(F32)
-    stream = (res_ref[:, at(t * col, col)].astype(F32) + attended).astype(BF16).astype(F32)
+    stream = (res_ref[...].astype(F32) + attended).astype(BF16).astype(F32)
     stream_s[...] = stream
     squares = jnp.sum(stream * stream, axis=1, keepdims=True)
     sums[...] = jnp.broadcast_to(squares, (rows, 128)).T[0:8, :]
-    for d in range(n_tp - 1):
+    for d in range(far):
         sum_copy(d).start()
     square_row = sums[0:1, :]
-    for d in range(n_tp - 1):
+    for d in range(far):
         sum_copy(d).wait_recv()
         square_row = square_row + sums_in[d, 0:1, :]
     squares = jnp.broadcast_to(square_row, (128, rows)).T[:, 0:1]
     normed = (
-        stream * lax.rsqrt(squares * (1.0 / width) + epsilon) * gain_ref[0:1, at(t * col, col)]
+        stream * lax.rsqrt(squares * (1.0 / width) + epsilon) * gain_ref[0:1, own]
     ).astype(BF16)
-    first, second = tgt_rows_ref[0:1, :], tgt_rows_ref[1:2, :]
     slot_in = lax.broadcasted_iota(jnp.int32, (cap, rows), 0)
 
     def dispatch(e):
         slots = slot_in + e * cap
-        pick = ((first == slots) | (second == slots)).astype(F32).astype(BF16)
+        pick = ((tgt_rows[0] == slots) | (tgt_rows[1] == slots)).astype(F32).astype(BF16)
         return dot_f32(pick, normed).astype(BF16)
 
-    for dst in sp_others:
+    arrived[t, at(s * cap, cap), :] = dispatch(s)
+    partner = s + 1 - 2 * lax.rem(s, 2)
+    targets = [partner]
+    for k in range(1, groups):
+        there = lax.rem(chip + groups - k, groups)
+        targets += [2 * there, 2 * there + 1]
+    for dst in targets:
         outgoing[at(dst * cap, cap), :] = dispatch(dst)
         out_copy(dst, s).start()
-    arrived[t, at(s * cap, cap), :] = dispatch(s)
-    for load in loads:
-        load.wait()
-    chip = s // 2
+
+    def group_of(k):
+        return lax.rem(chip + k, groups)
 
     def relay(k):
-        g = lax.rem(chip + k, groups)
+        g = group_of(k)
         for core in range(2):
             src = 2 * g + core
 
@@ -418,13 +459,19 @@
             def _():
                 out_copy(src, src).wait_recv()
 
-        for d in range(n_tp - 1):
-            ag_copy(d, g).start()
+        for d in range(2):
+            ag_copy(d, g, t).start()
+
+    def forward(k):
+        g = group_of(k)
+        for d in range(2):
+            ag_copy(d, g, peers[d]).wait_recv()
+            fw_copy(d, g, peers[d]).start()
 
     def compute(k):
-        g = lax.rem(chip + k, groups)
-        for d in range(n_tp - 1):
-            ag_wait(d, g)
+        g = group_of(k)
+        for d in range(2):
+            fw_copy(d, g, corner).wait_recv()
         ff = gate_w.shape[1]
         tile = min(256, ff)
         here = at(g * span, span)
@@ -442,21 +489,38 @@
             return carry
 
         lax.fori_loop(0, ff // tile, hidden_tile, 0)
-        for d in range(n_tp - 1):
-            parts[d, here, :] = dot_f32(
-                hidden[...], down_w[:, at(tp_others[d] * col, col)]
+
+        def part(place, owner):
+            parts[place, here, :] = dot_f32(
+                hidden[...], down_w[:, at(owner * col, col)]
             ).astype(BF16)
-            part_copy(d, g).start()
-        parts[n_tp - 1, here, :] = dot_f32(hidden[...], down_w[:, at(t * col, col)]).astype(BF16)
+
+        part(3, corner)
+        mid_copy(0, g).start()
+        mid_copy(1, g).start()
+        part(1, beside)
+        part_copy(0, 0, g).start()
+        part(2, across)
+        part_copy(1, 1, g).start()
+        part(0, t)
+
+    def add(k):
+        g = group_of(k)
+        for d in range(2):
+            mid_copy(d, g).wait_recv()
+            here = at((2 * g + d) * cap, cap)
+            both = parts[2 - d, here, :].astype(F32) + mid[d, at(g * cap, cap), :].astype(F32)
+            parts[2 - d, here, :] = both.astype(BF16)
+            part_copy(1 - d, d, g).start()
 
     def finish(k):
-        g = lax.rem(chip + k, groups)
+        g = group_of(k)
         here = at(g * span, span)
-        total = parts[n_tp - 1, here, :].astype(F32)
-        for d in range(n_tp - 1):
-            part_copy(d, g).wait_recv()
-            total = total + parts_in[d, here, :].astype(F32)
-        ret[here, :] = total.astype(BF16)
+        for d in range(2):
+            for half in range(2):
+                part_copy(d, half, g).wait_recv()
+        total = parts[0, here, :].astype(F32) + parts_in[0, here, :].astype(F32)
+        ret[here, :] = (total + parts_in[1, here, :].astype(F32)).astype(BF16)
         for core in range(2):
             src = 2 * g + core
 
@@ -465,34 +529,48 @@
                 ret_copy(src, s).start()
 
     relay(0)
+    relay(1)
+    forward(0)
+    for load in loads[2:]:
+        load.wait()
 
     def step(k, carry):
+        @pl.when(k + 2 < groups)
+        def _():
+            relay(k + 2)
+
+        compute(k)
+
         @pl.when(k + 1 < groups)
         def _():
-            relay(k + 1)
-
-        compute(k)
+            forward(k + 1)
 
         @pl.when(k > 0)
         def _():
-            finish(k - 1)
+            add(k - 1)
+
+        @pl.when(k > 1)
+        def _():
+            finish(k - 2)
 
         return carry
 
     lax.fori_loop(0, groups, step, 0)
+    add(groups - 1)
+    finish(groups - 2)
     finish(groups - 1)
     ret_in[at(s * cap, cap), :] = ret[at(s * cap, cap), :]
     for dst in sp_others:
         ret_copy(dst, dst).wait_recv()
     slots = lax.broadcasted_iota(jnp.int32, (rows, n_sp * cap), 1)
+    gap = jnp.broadcast_to(scores_ref[1:2, :] - scores_ref[0:1, :], (128, rows)).T[:, 0:1]
+    shares = (1.0 / (1.0 + jnp.exp(gap)), 1.0 / (1.0 + jnp.exp(-gap)))
     total = jnp.zeros((rows, col), F32)
     for k in range(2):
-        pick = (tgt_cols_ref[:, k : k + 1] == slots).astype(F32).astype(BF16)
-        other = share_ref[:, 1 - k : 2 - k]
-        share = 1.0 / (1.0 + jnp.exp(other - share_ref[:, k : k + 1]))
-        total = total + dot_f32(pick, ret_in[...]) * share
+        pick = (tgt_cols[k] == slots).astype(F32).astype(BF16)
+        total = total + dot_f32(pick, ret_in[...]) * shares[k]
     out_ref[...] = (stream_s[...] + total).astype(BF16)
-    for d in range(n_tp - 1):
+    for d in range(far):
         term_copy(d).wait_send()
         sum_copy(d).wait_send()
     for dst in sp_others:
@@ -500,9 +578,12 @@
         ret_copy(dst, s).wait_send()
 
     def drain(g, carry):
-        for d in range(n_tp - 1):
-            ag_copy(d, g).wait_send()
-            part_copy(d, g).wait_send()
+        for d in range(2):
+            ag_copy(d, g, t).wait_send()
+            fw_copy(d, g, peers[d]).wait_send()
+            mid_copy(d, g).wait_send()
+            for half in range(2):
+                part_copy(d, half, g).wait_send()
         return carry
 
     lax.fori_loop(0, groups, drain, 0)
@@ -528,58 +609,59 @@
     cap = 4 * rows // n_sp
     slots = n_sp * cap
     ff = gate_weight.shape[2]
-    mixed = attend_by_head(n_sp, queries, keys, values).reshape(n_sp * HD, rows)
-    targets = route_targets(expert_routes, n_sp, cap).reshape(rows, 2)
     anywhere = pl.BlockSpec(memory_space=pl.ANY)
     dma = pltpu.SemaphoreType.DMA
     far = n_tp - 1
     groups = n_sp // 2
+    held = [
+        (n_sp, 3 * HD, rows),
+        (n_sp, 3 * HD, rows),
+        (n_sp, HD, rows),
+        (n_sp, HD, rows),
+    ]
+    moved = [
+        (out_weight.shape, BF16),
+        ((rows, col), BF16),
+        ((width, ff), BF16),
+        ((width, ff), BF16),
+        ((ff, width), BF16),
+        ((far, rows, col), BF16),
+        ((far, rows, col), BF16),
+        ((8, rows), F32),
+        ((far, 8, rows), F32),
+        ((slots, col), BF16),
+        ((n_tp, slots, col), BF16),
+        ((2 * cap, ff), BF16),
+        ((n_tp, slots, col), BF16),
+        ((2, slots // 2, col), BF16),
+        ((2, slots, col), BF16),
+        ((slots, col), BF16),
+        ((slots, col), BF16),
+        ((rows, col), F32),
+    ]
+    counts = [(5,)] + [(far,)] * 4 + [(n_sp,)] * 2 + [(2, groups)] * 6
+    counts += [(2, 2, groups)] * 2 + [(n_sp,)] * 2
     return pl.pallas_call(
         functools.partial(expert_kernel, n_sp, n_tp),
         out_shape=jax.ShapeDtypeStruct((rows, col), BF16),
-        in_specs=[VM] * 7 + [anywhere] * 3,
+        in_specs=[VM] * 6 + [anywhere] * 5,
         out_specs=VM,
-        scratch_shapes=[
-            pltpu.VMEM((width, ff), BF16),
-            pltpu.VMEM((width, ff), BF16),
-            pltpu.VMEM((ff, width), BF16),
-            pltpu.VMEM((far, rows, col), BF16),
-            pltpu.VMEM((far, rows, col), BF16),
-            pltpu.VMEM((8, rows), F32),
-            pltpu.VMEM((far, 8, rows), F32),
-            pltpu.VMEM((slots, col), BF16),
-            pltpu.VMEM((n_tp, slots, col), BF16),
-            pltpu.VMEM((2 * cap, ff), BF16),
-            pltpu.VMEM((n_tp, slots, col), BF16),
-            pltpu.VMEM((far, slots, col), BF16),
-            pltpu.VMEM((slots, col), BF16),
-            pltpu.VMEM((slots, col), BF16),
-            pltpu.VMEM((rows, col), F32),
-            dma((3,)),
-            dma((far,)),
-            dma((far,)),
-            dma((far,)),
-            dma((far,)),
-            dma((n_sp,)),
-            dma((n_sp,)),
-            dma((far, groups)),
-            dma((far, groups)),
-            dma((far, groups)),
-            dma((far, groups)),
-            dma((n_sp,)),
-            dma((n_sp,)),
-        ],
+        scratch_shapes=[pltpu.VMEM(shape, BF16) for shape in held]
+        + [dma((n_sp,))] * 4
+        + [pltpu.VMEM(shape, kind) for shape, kind in moved]
+        + [dma(count) for count in counts],
         compiler_params=pltpu.CompilerParams(
-            collective_id=1, has_side_effects=True, vmem_limit_bytes=60 * 1024 * 1024
+            collective_id=0, has_side_effects=True, vmem_limit_bytes=60 * 1024 * 1024
         ),
     )(
-        mixed,
+        queries,
+        keys,
+        values,
+        expert_routes.T,
+        route_scores.T,
+        norm_gain.reshape(1, width),
         out_weight,
         residual_in,
-        norm_gain.reshape(1, width),
-        targets.T,
-        targets,
-        route_scores,
         gate_weight[0],
         up_weight[0],
         down_weight[0],
@@ -605,7 +687,7 @@
 
     def body(*args):
         heads = args[1].shape[1] // HD
-        if heads == n_sp:
+        if heads == n_sp and n_tp == 4 and n_sp % 4 == 0 and n_sp <= 128:
             return fused_shards(n_sp, n_tp, *args)
         return shards(*args)
 

time: 189 us -> 152 us (0.80)
  Pallas kernels: 179 us -> 149 us
  local copies, waits for them, and re-layouts: 5.37 us -> 1.67 us
  other arithmetic: 1.98 us -> 0 us
    pallas_call x1 -> x0, Pallas kernels: 38.5 us -> none  [attend_by_head(): pl.pallas_call(functools.partial(attention_kernel, n), out_shape=jax.Shap...]
    pallas_call x1, Pallas kernels: 141 us -> 149 us  [fused_shards(): pl.pallas_call(functools.partial(expert_kernel, n_sp, n_tp), out_shape=ja...]
    unnamed x5 -> x1, local copies, waits for them, and re-layouts: 3.96 us -> 1.67 us
where the time goes in v2:
time: 152 us; the launch traced here: 151 us
  Pallas kernels  149 us (98%)
  local copies, waits for them, and re-layouts  1.67 us (1%)
    pallas_call x1, Pallas kernels, fused_shards(): pl.pallas_call(functools.partial(expert_kernel, n_sp, n_tp), out_shape=ja...  149 us

profile of v2, /device:TPU:0, one launch (start us, length us, event | category | flops | bytes accessed | tf_op | source)
XLA Modules:
  0.0 150.5 jit_solution(11669494820795047638)
XLA Ops:
  0.0 148.8 %shard_map.109 = bf16[256,512]{1,0:T(8,128)(2,1)} custom-call(bf16[256,512]{1,0:T(8,128)(2,1)} %q_ref.1, bf16[256,512]{1,0:T(8,128)(2,1)} %k_ref.1, bf16[256,512]{1,0:T(8,128)(2,1)} %v_ref.1, s32[2,256]{1,0:T(2,128)} %bitcast.10, f32[2,256]{1,0:T(2,128)} %bitcast.11, f32[1,2048]{1,0:T(1,128)} %bitcast.9, bf16[512,2048]{1,0:T(8,128)(2,1)} %ow_hbm.1, ...), custom_call_target="tpu_custom_call" | custom-call | tf_op jit(solution)/shard_map/pallas_call | solution.py:644
  148.9 1.7 %copy.13 = bf16[256,512]{1,0:T(8,128)(2,1)} copy(bf16[256,512]{1,0:T(8,128)(2,1)} %shard_map.109) | data formatting | bytes 524288
